TPU v7x, 32 devices: a whole 2x2x4 slice. The times are simulated.
32 devices in a mesh: ep: 8 (over z, core), tp: 4 (over y, x).
Axes of the slice: x: 2, y: 2, z: 4, core: 2. Of those that a mesh axis runs over, the one named last changes fastest.
Arguments:
- query_vectors: bfloat16 [4096, 4096], P('ep', 'tp'), may hold values from -6 to 6
- key_vectors: bfloat16 [4096, 2048], P('ep', 'tp'), may hold values from -6 to 6
- value_vectors: bfloat16 [4096, 2048], P('ep', 'tp'), may hold values from -64 to 64
- query_gain: float32 [128], replicated, may hold values from 0.1 to 1.9
- key_gain: float32 [128], replicated, may hold values from 0.1 to 1.9
- sink_logits: float32 [32], P('tp'), may hold values from 3 to 7
- moe_rows: bfloat16 [1280, 4096], P('ep', 'tp'), may hold values from -6 to 6
- norm_gain: float32 [4096], replicated, may hold values from 0.1 to 1.9
- expert_ids: int32 [1280, 4], P('ep'), may hold values from 0 to 7, all different within a row; in each aligned block of 160 rows (0 to 159, 160 to 319, ...) at most 120 rows name the same one
- route_weights: float32 [1280, 4], P('ep'), may hold values from 0.25 to 2.5
- expert_gate: bfloat16 [8, 4096, 2048], P('ep', None, 'tp'), may hold values from -0.09375 to 0.09375
- expert_up: bfloat16 [8, 4096, 2048], P('ep', None, 'tp'), may hold values from -0.09375 to 0.09375
- expert_down: bfloat16 [8, 2048, 4096], P('ep', None, 'tp'), may hold values from -0.125 to 0.125
- shared_gate: bfloat16 [4096, 512], P(None, 'tp'), may hold values from -0.09375 to 0.09375
- shared_up: bfloat16 [4096, 512], P(None, 'tp'), may hold values from -0.09375 to 0.09375
- shared_down: bfloat16 [512, 4096], P(None, 'tp'), may hold values from -0.25 to 0.25
Outputs:
- attended: bfloat16 [4096, 4096], P('ep', 'tp')
- moe_out: bfloat16 [1280, 4096], P('ep', 'tp')
Inputs may be any that keep to these rules, and one draw needn't show every extreme that they name: `expert_ids`: each row names 4 different experts. Within the rows of one index of ep (aligned blocks of 160 rows), no expert is named by more than 120 rows, and in some block one expert is named by exactly 120.
All inputs are finite; a program needn't handle non-finite values.
Results may differ from a plain program's by a relative error of at most 0.0071.
Values may be sent and summed in bfloat16 or wider, within the bound.
A program may use at most 128 MiB of HBM per device.

v0:
```python
import jax
import jax.numpy as jnp
from jax import lax
from jax.sharding import PartitionSpec as P

HEAD_DIM = 128
WINDOW = 128
GRID_W = 64
D = 4096
TOP_K = 4


epsilon = 1e-06
rotary_base = 10000.0


def padded_2(block, sides, width):
    for axis, dim in sides:
        count = lax.axis_size(axis)
        forward = [(i, i + 1) for i in range(count - 1)]
        backward = [(target, source) for source, target in forward]
        low = lax.ppermute(
            lax.slice_in_dim(block, block.shape[dim] - width, None, axis=dim), axis, forward
        )
        high = lax.ppermute(lax.slice_in_dim(block, 0, width, axis=dim), axis, backward)
        block = jnp.concatenate([low, block, high], axis=dim)
    return block


def half_turn(halves):
    leading, trailing = jnp.split(halves, 2, axis=-1)
    return jnp.concatenate([-trailing, leading], axis=-1)


def rotate_heads(vectors, head_gain, positions):
    floats = vectors.astype(jnp.float32)
    normed = (
        floats * lax.rsqrt(jnp.mean(floats * floats, axis=-1, keepdims=True) + epsilon) * head_gain
    )
    quarter = HEAD_DIM // 4
    freq_index = jnp.arange(quarter, dtype=jnp.int32).astype(jnp.float32)
    inverse = rotary_base ** (-4.0 * freq_index / HEAD_DIM)
    grid_row = (positions // GRID_W).astype(jnp.float32)[:, None] * inverse
    grid_col = (positions % GRID_W).astype(jnp.float32)[:, None] * inverse
    angles = jnp.concatenate([grid_row, grid_row, grid_col, grid_col], axis=-1)[:, None, :]
    row_half, col_half = jnp.split(normed, 2, axis=-1)
    turned = jnp.concatenate([half_turn(row_half), half_turn(col_half)], axis=-1)
    return (normed * jnp.cos(angles) + turned * jnp.sin(angles)).astype(jnp.bfloat16)


def attend_window(query_vectors, key_vectors, value_vectors, query_gain, key_gain, sink_logits):
    length = query_vectors.shape[0]
    heads_here = sink_logits.shape[0]
    kv_here = key_vectors.shape[1] // HEAD_DIM
    grouping = heads_here // kv_here
    shard_start = lax.axis_index("ep") * length
    positions = shard_start + jnp.arange(length, dtype=jnp.int32)
    queries = rotate_heads(
        query_vectors.reshape(length, heads_here, HEAD_DIM), query_gain, positions
    )
    turned_keys = rotate_heads(key_vectors.reshape(length, kv_here, HEAD_DIM), key_gain, positions)
    turned_keys = turned_keys.reshape(length, kv_here * HEAD_DIM)
    padded = padded_2(jnp.stack([turned_keys, value_vectors]), (("ep", 1),), WINDOW)
    extent = length + 2 * WINDOW
    near_keys = padded[0].reshape(extent, kv_here, HEAD_DIM)
    near_values = padded[1].reshape(extent, kv_here, HEAD_DIM)
    key_pos = shard_start - WINDOW + jnp.arange(extent, dtype=jnp.int32)
    inside = (
        (jnp.abs(positions[:, None] - key_pos[None, :]) <= WINDOW)
        & (key_pos >= 0)[None, :]
        & (key_pos < lax.axis_size("ep") * length)[None, :]
    )
    scores = jnp.einsum(
        "qhgd,khd->hgqk",
        queries.reshape(length, kv_here, grouping, HEAD_DIM),
        near_keys,
        preferred_element_type=jnp.float32,
    ) * HEAD_DIM ** (-0.5)
    raised = jnp.where(inside, jnp.exp(scores), 0.0)
    denominator = jnp.exp(sink_logits).reshape(kv_here, grouping)[:, :, None] + jnp.sum(
        raised, axis=-1
    )
    weights = (raised / denominator[..., None]).astype(jnp.bfloat16)
    mixed = jnp.einsum("hgqk,khd->qhgd", weights, near_values, preferred_element_type=jnp.float32)
    return mixed.astype(jnp.bfloat16).reshape(length, heads_here * HEAD_DIM)


def project(block_rows, gain_piece, gate_rows, up_rows):
    floats = block_rows.astype(jnp.float32)
    weighted = (floats * gain_piece).astype(jnp.bfloat16)
    gate_sum = jnp.dot(weighted, gate_rows, preferred_element_type=jnp.float32)
    up_sum = jnp.dot(weighted, up_rows, preferred_element_type=jnp.float32)
    return (gate_sum, up_sum, jnp.sum(floats * floats, axis=1))


def activate(gate_sum, up_sum, squares):
    factor = lax.rsqrt(squares / D + epsilon)[:, None]
    return (jax.nn.silu(gate_sum * factor) * (up_sum * factor)).astype(jnp.bfloat16)


def shards(
    query_vectors,
    key_vectors,
    value_vectors,
    query_gain,
    key_gain,
    sink_logits,
    moe_rows,
    norm_gain,
    expert_ids,
    route_weights,
    expert_gate,
    expert_up,
    expert_down,
    shared_gate,
    shared_up,
    shared_down,
):
    attended = attend_window(
        query_vectors, key_vectors, value_vectors, query_gain, key_gain, sink_logits
    )
    ep_size = lax.axis_size("ep")
    tokens_here, width_here = moe_rows.shape
    capacity = max(2, 3 * tokens_here * TOP_K // (2 * ep_size))
    slots_all = ep_size * capacity
    flat_ids = expert_ids.reshape(-1)
    onehot = (flat_ids[:, None] == jnp.arange(ep_size, dtype=jnp.int32)[None, :]).astype(jnp.int32)
    slot_index = jnp.sum((jnp.cumsum(onehot, axis=0) - onehot) * onehot, axis=1)
    target = flat_ids * capacity + slot_index
    matches = target[None, :] == jnp.arange(slots_all, dtype=jnp.int32)[:, None]
    present = jnp.any(matches, axis=1)
    owner_row = jnp.arange(tokens_here * TOP_K, dtype=jnp.int32) // TOP_K
    source_row = jnp.sum(jnp.where(matches, owner_row[None, :], 0), axis=1)
    local_gate = expert_gate[0]
    local_up = expert_up[0]
    local_down = expert_down[0]
    units_here = local_gate.shape[1]
    shared_units = shared_gate.shape[1]
    outgoing = jnp.where(
        present[:, None], jnp.take(moe_rows, source_row, axis=0), jnp.zeros((), jnp.bfloat16)
    )
    arrived = lax.all_to_all(
        outgoing.reshape(ep_size, capacity, width_here),
        "ep",
        split_axis=0,
        concat_axis=0,
        tiled=True,
    )
    arrived = arrived.reshape(slots_all, width_here)
    routed = project(
        lax.all_gather(arrived, "tp", axis=1, tiled=True), norm_gain, local_gate, local_up
    )
    shared = project(
        lax.all_gather(moe_rows, "tp", axis=1, tiled=True), norm_gain, shared_gate, shared_up
    )
    gate_sum, up_sum, squares, shared_gsum, shared_usum, own_squares = tuple(
        (new_term for new_term in routed + shared)
    )
    hidden = activate(gate_sum, up_sum, squares)
    shared_hidden = activate(shared_gsum, shared_usum, own_squares)
    packing = units_here // shared_units
    stacked = jnp.concatenate(
        [hidden, shared_hidden.reshape(tokens_here // packing, units_here)], axis=0
    )
    columns = local_down.shape[1]
    portion = lax.all_gather(stacked, "tp", axis=1, tiled=True)
    shards_in = portion.shape[1] // units_here
    routed = jnp.dot(portion[:slots_all], local_down, preferred_element_type=jnp.float32)
    shared_piece = portion[slots_all:].reshape(
        tokens_here // packing, shards_in, packing, shared_units
    )
    shared_piece = shared_piece.transpose(0, 2, 1, 3).reshape(tokens_here, shards_in * shared_units)
    shared = jnp.dot(shared_piece, shared_down, preferred_element_type=jnp.float32)
    returned = lax.all_to_all(
        routed.astype(jnp.bfloat16).reshape(ep_size, capacity, columns),
        "ep",
        split_axis=0,
        concat_axis=0,
        tiled=True,
    )
    returned = returned.reshape(slots_all, columns)
    picked = jnp.take(returned, target, axis=0).reshape(tokens_here, TOP_K, columns)
    combined = shared + jnp.sum(route_weights[:, :, None] * picked.astype(jnp.float32), axis=1)
    return (attended, combined.astype(jnp.bfloat16))


def solution(mesh):
    placed = (
        P("ep", "tp"),
        P("ep", "tp"),
        P("ep", "tp"),
        P(),
        P(),
        P("tp"),
        P("ep", "tp"),
        P(),
        P("ep", None),
        P("ep", None),
        P("ep", None, "tp"),
        P("ep", None, "tp"),
        P("ep", None, "tp"),
        P(None, "tp"),
        P(None, "tp"),
        P(None, "tp"),
    )
    return jax.shard_map(
        shards,
        mesh=mesh,
        in_specs=placed,
        out_specs=(P("ep", "tp"), P("ep", "tp")),
        check_vma=False,
    )
```

profile of v0, /device:TPU:0, one launch (start us, length us, event | category | flops | bytes accessed | tf_op | source)
XLA Modules:
  0.0 298.6 jit_solution(4147302405466254535)
XLA Ops:
  11.2 4.2 %gather_fusion = bf16[960,1024]{1,0:T(8,128)(2,1)S(1)} fusion(bf16[160,1024]{1,0:T(8,128)(2,1)S(1)} %copy-done.1, s32[1024]{0:T(1024)S(1)} %pad_clamp_fusion.1), kind=kCustom, calls=%fused_computation | custom fusion | bytes 3936000 | tf_op jit(solution)/shard_map/jit(_take)/gather | solution.py:140
  16.9 6.4 %all-to-all-start = ((bf16[8,120,1024]{2,1,0:T(8,128)(2,1)}), bf16[8,120,1024]{2,1,0:T(8,128)(2,1)S(1)}, u32[]{:S(2)}, u32[]{:S(2)}) async-start(bf16[8,120,1024]{2,1,0:T(8,128)(2,1)} %select_select_fusion), calls=%async_computation | async-start | bytes 3932160 | tf_op jit(solution)/shard_map/all_to_all | solution.py:142
  24.0 45.4 %all-to-all-done = bf16[8,120,1024]{2,1,0:T(8,128)(2,1)S(1)} async-done(((bf16[8,120,1024]{2,1,0:T(8,128)(2,1)}), bf16[8,120,1024]{2,1,0:T(8,128)(2,1)S(1)}, u32[]{:S(2)}, u32[]{:S(2)}) %all-to-all-start) | async-done | bytes 1966112 | tf_op jit(solution)/shard_map/all_to_all | solution.py:142
  72.8 2.1 fusion.37
  75.4 77.6 %all-gather.4.cloned.1.call-done = bf16[960,4096]{1,0:T(8,128)(2,1)} async-done(((bf16[960,1024]{1,0:T(8,128)(2,1)}), bf16[960,4096]{1,0:T(8,128)(2,1)}) %all-gather.4.cloned.1.call-update) | async-done | bytes 7864336 | tf_op jit(solution)/shard_map/all_gather | solution.py:151
  153.1 5.0 %fusion.1 = f32[960]{0:T(1024)S(1)} fusion(bf16[960,4096]{1,0:T(8,128)(2,1)} %all-gather.4.cloned.1.call-done), kind=kLoop, calls=%fused_computation.5 | loop fusion | flops 11795520 | bytes 7868160 | tf_op jit(solution)/shard_map/reduce_sum | solution.py:93
  158.5 6.4 %fusion.3 = f32[960,512]{1,0:T(8,128)S(1)} fusion(bf16[960,4096]{1,0:T(8,128)(2,1)S(1)} %copy-done.5, f32[4096]{0:T(1024)S(1)} %copy-done.27, bf16[1,4096,512]{2,1,0:T(8,128)(2,1)} %param.27), kind=kOutput, calls=%fused_computation.9 | convolution fusion | flops 4038328320 | bytes 14041088 | tf_op jit(solution)/shard_map/dot_general | solution.py:92
  165.0 4.6 %multiply_convert_fusion = bf16[960,512]{1,0:T(8,128)(2,1)S(1)} fusion(f32[960,512]{1,0:T(8,128)S(1)} %fusion.3, bf16[1,4096,512]{2,1,0:T(8,128)(2,1)S(1)} %copy-done.25, bf16[960,4096]{1,0:T(8,128)(2,1)S(1)} %copy-done.5, f32[4096]{0:T(1024)S(1)} %copy-done.27, f32[960]{0:T(1024)S(1)} %add_rsqrt_fusion.2), kind=kOutput, calls=%fused_computation.33 | convolution fusion | flops 4042260480 | bytes 15027968 | tf_op jit(solution)/shard_map/dot_general | solution.py:91
  176.4 3.7 %collective-permute-start = (bf16[2,128,512]{1,2,0:T(8,128)(2,1)}, bf16[2,128,512]{1,2,0:T(8,128)(2,1)}, u32[]{:S(2)}, u32[]{:S(2)}) collective-permute-start(bf16[2,128,512]{1,2,0:T(8,128)(2,1)} %get-tuple-element.18), channel_id=1, source_target_pairs={{0,4},{4,8},{8,12},{12,16},{16,20},{20,24},{24,28},{1,5},{5,9},{9,... | collective-permute-start | bytes 786440 | tf_op jit(solution)/shard_map/ppermute | solution.py:22
  181.6 4.2 %reshape.381 = f32[512,4,2,128]{3,2,1,0:T(2,128)} reshape(bf16[512,1024]{1,0:T(8,128)(2,1)} %param.16) | data formatting | bytes 3145728 | tf_op jit(solution)/shard_map/convert_element_type | solution.py:36
  187.0 2.0 copy.80
  189.0 1.9 copy.79
  190.9 1.9 copy.78
  192.8 1.9 copy.77
  199.3 23.1 %all-gather.8.cloned.1.call-done = bf16[1000,2048]{1,0:T(8,128)(2,1)} async-done(((bf16[1000,512]{1,0:T(8,128)(2,1)}), bf16[1000,2048]{1,0:T(8,128)(2,1)}) %all-gather.8.cloned.1.call-update) | async-done | bytes 4096016 | tf_op jit(solution)/shard_map/all_gather | solution.py:166
  222.4 8.9 %fusion.20 = bf16[960,1024]{1,0:T(8,128)(2,1)} fusion(bf16[1,2048,1024]{2,1,0:T(8,128)(2,1)} %param.28, bf16[1000,2048]{1,0:T(8,128)(2,1)} %all-gather.8.cloned.1.call-done), kind=kOutput, calls=%fused_computation.35 | convolution fusion | flops 4027514880 | bytes 10092544 | tf_op jit(solution)/shard_map/dot_general | solution.py:168
  231.3 4.7 %all-to-all-start.1 = ((bf16[8,120,1024]{2,1,0:T(8,128)(2,1)}), bf16[8,120,1024]{2,1,0:T(8,128)(2,1)S(1)}, u32[]{:S(2)}, u32[]{:S(2)}) async-start(bf16[8,120,1024]{2,1,0:T(8,128)(2,1)} %bitcast.104), calls=%async_computation.1 | async-start | bytes 3932160 | tf_op jit(solution)/shard_map/all_to_all | solution.py:174
  240.7 7.2 %fusion.2 = (f32[4,2,512]{2,1,0:T(2,128)S(1)}, f32[4,768,512,2]{2,1,3,0:T(8,128)S(1)}) fusion(pred[512,768]{0,1:T(8,128)(4,1)} %fusion.30, bf16[768,4,128,1]{0,2,3,1:T(8,128)(2,1)S(1)} %bitcast.99, f32[512,4,2,32]{3,0,2,1:T(8,128)S(1)} %copy-done.2, f32[512,4,2,32]{3,0,2,1:T(8,128)S(1)} %copy-done.3, f32[512,4,2,32]{3,0,2,1:T(8,128)S(1)} %copy-done.4, ...), kind=kOutput, calls=%fused_computation.8 | convolution fusion | flops 819458048 | bytes 18514432 | tf_op jit(solution)/shard_map/qhgd,khd->hgqk/dot_general | solution.py:73
  248.0 4.2 %fusion.31 = bf16[4,128,2,512]{3,1,2,0:T(8,128)(2,1)} fusion(bf16[768,4,128,1]{0,2,3,1:T(8,128)(2,1)S(1)} %bitcast.106, f32[4,768,512,2]{2,1,3,0:T(8,128)S(1)} %get-tuple-element.29, f32[4,2,512]{2,1,0:T(2,128)S(1)} %broadcast_add_fusion, pred[512,768]{0,1:T(8,128)(4,1)S(1)} %copy-done.12), kind=kOutput, calls=%fused_computation.40 | convolution fusion | flops 818413568 | bytes 14827520 | tf_op jit(solution)/shard_map/hgqk,khd->qhgd/dot_general | solution.py:84
  252.2 2.3 copy.92
  254.7 27.6 %all-to-all-done.1 = bf16[8,120,1024]{2,1,0:T(8,128)(2,1)S(1)} async-done(((bf16[8,120,1024]{2,1,0:T(8,128)(2,1)}), bf16[8,120,1024]{2,1,0:T(8,128)(2,1)S(1)}, u32[]{:S(2)}, u32[]{:S(2)}) %all-to-all-start.1) | async-done | bytes 1966112 | tf_op jit(solution)/shard_map/all_to_all | solution.py:174
  282.2 3.5 %gather_fusion.1 = bf16[640,1024]{1,0:T(8,128)(2,1)} fusion(bf16[960,1024]{1,0:T(8,128)(2,1)S(1)} %bitcast.92, s32[1024]{0:T(1024)S(1)} %copy-done.19), kind=kCustom, calls=%fused_computation.1 | custom fusion | bytes 2624000 | tf_op jit(solution)/shard_map/jit(_take)/gather | solution.py:182
  285.7 2.6 gather.15
  288.4 2.6 multiply_reduce_fusion
  (139 shorter events, 30.2 us)
Async XLA Ops:
  7.2 283.8 %copy-start = (bf16[512,1024]{1,0:T(8,128)(2,1)S(1)}, bf16[512,1024]{1,0:T(8,128)(2,1)}, u32[]{:S(2)}) copy-start(bf16[512,1024]{1,0:T(8,128)(2,1)} %param.31) | copy-start | bytes 3145732
  7.2 4.0 %copy-start.1 = (bf16[160,1024]{1,0:T(8,128)(2,1)S(1)}, bf16[160,1024]{1,0:T(8,128)(2,1)}, u32[]{:S(2)}) copy-start(bf16[160,1024]{1,0:T(8,128)(2,1)} %param.22) | copy-start | bytes 983044
  16.9 52.6 %all-to-all-start = ((bf16[8,120,1024]{2,1,0:T(8,128)(2,1)}), bf16[8,120,1024]{2,1,0:T(8,128)(2,1)S(1)}, u32[]{:S(2)}, u32[]{:S(2)}) async-start(bf16[8,120,1024]{2,1,0:T(8,128)(2,1)} %select_select_fusion), calls=%async_computation | async-start | bytes 3932160 | tf_op jit(solution)/shard_map/all_to_all | solution.py:142
  23.3 49.5 %copy-start.27 = (f32[4096]{0:T(1024)S(1)}, f32[4096]{0:T(1024)}, u32[]{:S(2)}) copy-start(f32[4096]{0:T(1024)} %param.23) | copy-start | bytes 49156
  23.3 47.7 %all-gather.6.cloned.1.call-start = ((), (), s32[]{:S(2)}) async-start(), calls=%async_computation.3 | async-start | bytes 1638400 | tf_op jit(solution)/shard_map/all_gather | solution.py:154
  24.0 129.1 %all-gather.4.cloned.1.call-start = ((), (), s32[]{:S(2)}) async-start(), calls=%async_computation.2 | async-start | bytes 9830400 | tf_op jit(solution)/shard_map/all_gather | solution.py:151
  70.8 4.0 %copy-start.26 = (bf16[4096,128]{1,0:T(8,128)(2,1)S(1)}, bf16[4096,128]{1,0:T(8,128)(2,1)}, u32[]{:S(2)}) copy-start(bf16[4096,128]{1,0:T(8,128)(2,1)} %param.30) | copy-start | bytes 3145732
  70.9 151.5 %all-gather.8.cloned.1.call-start = ((), (), s32[]{:S(2)}) async-start(), calls=%async_computation.4 | async-start | bytes 5120000 | tf_op jit(solution)/shard_map/all_gather | solution.py:166
  70.9 4.0 %copy-start.13 = (bf16[160,4096]{1,0:T(8,128)(2,1)S(1)}, bf16[160,4096]{1,0:T(8,128)(2,1)}, u32[]{:S(2)}) copy-start(bf16[160,4096]{1,0:T(8,128)(2,1)} %all-gather.6.cloned.1.call-done) | copy-start | bytes 3932164
  153.1 5.5 %copy-start.5 = (bf16[960,4096]{1,0:T(8,128)(2,1)S(1)}, bf16[960,4096]{1,0:T(8,128)(2,1)}, u32[]{:S(2)}) copy-start(bf16[960,4096]{1,0:T(8,128)(2,1)} %all-gather.4.cloned.1.call-done) | copy-start | bytes 23592964
  158.5 6.4 %copy-start.25 = (bf16[1,4096,512]{2,1,0:T(8,128)(2,1)S(1)}, bf16[1,4096,512]{2,1,0:T(8,128)(2,1)}, u32[]{:S(2)}) copy-start(bf16[1,4096,512]{2,1,0:T(8,128)(2,1)} %param.26) | copy-start | bytes 12582916
  171.1 3.0 %copy-start.7 = (bf16[512,512]{0,1:T(8,128)(2,1)}, bf16[512,512]{0,1:T(8,128)(2,1)S(1)}, u32[]{:S(2)}) copy-start(bf16[512,512]{0,1:T(8,128)(2,1)S(1)} %copy.74) | copy-start | bytes 1572868
  175.1 62.2 %collective-permute-start.1 = (bf16[2,128,512]{1,2,0:T(8,128)(2,1)}, bf16[2,128,512]{1,2,0:T(8,128)(2,1)}, u32[]{:S(2)}, u32[]{:S(2)}) collective-permute-start(bf16[2,128,512]{1,2,0:T(8,128)(2,1)} %get-tuple-element.19), channel_id=1, source_target_pairs={{4,0},{8,4},{12,8},{16,12},{20,16},{24,20},{28,24},{5,1},{9,5},{13... | collective-permute-start | bytes 786440 | tf_op jit(solution)/shard_map/ppermute | solution.py:25
  176.4 60.9 %collective-permute-start = (bf16[2,128,512]{1,2,0:T(8,128)(2,1)}, bf16[2,128,512]{1,2,0:T(8,128)(2,1)}, u32[]{:S(2)}, u32[]{:S(2)}) collective-permute-start(bf16[2,128,512]{1,2,0:T(8,128)(2,1)} %get-tuple-element.18), channel_id=1, source_target_pairs={{0,4},{4,8},{8,12},{12,16},{16,20},{20,24},{24,28},{1,5},{5,9},{9,... | collective-permute-start | bytes 786440 | tf_op jit(solution)/shard_map/ppermute | solution.py:22
  181.6 4.6 %copy-start.21 = (f32[128]{0:T(128)S(1)}, f32[128]{0:T(128)}, u32[]{:S(2)}) copy-start(f32[128]{0:T(128)} %param.19) | copy-start | bytes 1540
  190.9 3.9 %copy-start.28 = (f32[8]{0:T(128)S(1)}, f32[8]{0:T(128)}, u32[]{:S(2)}) copy-start(f32[8]{0:T(128)} %param.21) | copy-start | bytes 100
  190.9 4.5 %copy-start.18 = (s32[160,4]{0,1:T(4,128)S(1)}, s32[160,4]{0,1:T(4,128)}, u32[]{:S(2)}) copy-start(s32[160,4]{0,1:T(4,128)} %param.24) | copy-start | bytes 7684
  190.9 4.8 %copy-start.23 = (f32[160,4]{0,1:T(4,128)S(1)}, f32[160,4]{0,1:T(4,128)}, u32[]{:S(2)}) copy-start(f32[160,4]{0,1:T(4,128)} %param.25) | copy-start | bytes 7684
  231.3 6.0 %copy-start.8 = (bf16[512,512]{0,1:T(8,128)(2,1)S(1)}, bf16[512,512]{0,1:T(8,128)(2,1)}, u32[]{:S(2)}) copy-start(bf16[512,512]{0,1:T(8,128)(2,1)} %copy-done.7) | copy-start | bytes 1572868
  231.3 51.0 %all-to-all-start.1 = ((bf16[8,120,1024]{2,1,0:T(8,128)(2,1)}), bf16[8,120,1024]{2,1,0:T(8,128)(2,1)S(1)}, u32[]{:S(2)}, u32[]{:S(2)}) async-start(bf16[8,120,1024]{2,1,0:T(8,128)(2,1)} %bitcast.104), calls=%async_computation.1 | async-start | bytes 3932160 | tf_op jit(solution)/shard_map/all_to_all | solution.py:174
  240.7 7.2 %copy-start.20 = (f32[4,2]{1,0:T(4,128)S(1)}, f32[4,2]{1,0:T(4,128)}, u32[]{:S(2)}) copy-start(f32[4,2]{1,0:T(4,128)} %add.209) | copy-start | bytes 100
  240.7 7.3 %copy-start.12 = (pred[512,768]{0,1:T(8,128)(4,1)S(1)}, pred[512,768]{0,1:T(8,128)(4,1)}, u32[]{:S(2)}) copy-start(pred[512,768]{0,1:T(8,128)(4,1)} %fusion.30) | copy-start | bytes 1179652
  252.2 30.0 %copy-start.19 = (s32[1024]{0:T(1024)S(1)}, s32[1024]{0:T(1024)}, u32[]{:S(2)}) copy-start(s32[1024]{0:T(1024)} %pad_clamp_fusion) | copy-start | bytes 12292
  285.7 2.7 copy-start.17
  (13 other events, 22.9 us)
Sparse Core Ops, SparseCore 0:
  25.9 30.1 all-gather.5
  71.0 82.0 all-gather.3
  170.7 51.6 all-gather.7
where the time goes:
time: 299 us
  waiting for transfers between devices  174 us (58%)
  local copies, waits for them, and re-layouts  35.3 us (12%)
  matrix products  34.9 us (12%)
  other arithmetic  23.4 us (8%)
  starting transfers between devices  16.2 us (5%)
  between operations  14.3 us (5%)
    all_gather x1, waiting for transfers between devices, shards(): lax.all_gather(arrived, 'tp', axis=1, tiled=True)  77.6 us
    all_to_all x1, waiting for transfers between devices, shards(): lax.all_to_all(outgoing.reshape(ep_size, capacity, width_here), 'ep', spl...  45.4 us
    all_to_all x1, waiting for transfers between devices, shards(): lax.all_to_all(routed.astype(jnp.bfloat16).reshape(ep_size, capacity, col...  27.6 us
    all_gather x1, waiting for transfers between devices, shards(): portion = lax.all_gather(stacked, 'tp', axis=1, tiled=True)  23.1 us
    dot_general x1, matrix products, shards(): jnp.dot(portion[:slots_all], local_down, preferred_element_type=jnp.float32)  8.88 us
    unnamed x63, local copies, waits for them, and re-layouts  8.45 us
    concatenate x4, local copies, waits for them, and re-layouts, rotate_heads(): jnp.concatenate([half_turn(row_half), half_turn(col_half)], axis=-1)  7.81 us
    dot_general x1, matrix products, attend_window(): jnp.einsum('qhgd,khd->hgqk', queries.reshape(length, kv_here, grouping, H...  7.16 us
  transfers between devices with their start and end apart: 7, of which 4 were waited for; matrix products, arithmetic and copies ran while one was open for 18% of the time, Pallas kernels for 0%

commit v1 on v0

--- a/solution.py
+++ b/solution.py
@@ -1,6 +1,10 @@
+import functools
+
 import jax
 import jax.numpy as jnp
 from jax import lax
+from jax.experimental import pallas as pl
+from jax.experimental.pallas import tpu as pltpu
 from jax.sharding import PartitionSpec as P
 
 HEAD_DIM = 128
@@ -184,6 +188,678 @@
     return (attended, combined.astype(jnp.bfloat16))
 
 
+F32 = jnp.float32
+BF16 = jnp.bfloat16
+MESH = pl.DeviceIdType.MESH
+LANES = 128
+
+
+def moe_kernel(
+    sizes,
+    q_hbm,
+    k_hbm,
+    v_hbm,
+    cos_ref,
+    sin_ref,
+    qgain_ref,
+    kgain_ref,
+    sink_ref,
+    x_hbm,
+    gain_ref,
+    wt_hbm,
+    gate_hbm,
+    up_hbm,
+    down_hbm,
+    sgate_hbm,
+    sup_hbm,
+    sdown_hbm,
+    att_ref,
+    out_ref,
+    xbuf,
+    gate,
+    up,
+    down,
+    sgate,
+    sup,
+    sdown,
+    qbuf,
+    kbuf,
+    vbuf,
+    wbuf,
+    scaled,
+    factor,
+    hid,
+    hbuf,
+    shbuf,
+    pbuf,
+    prx,
+    qtx,
+    qrx,
+    local_sem,
+    zs,
+    zr,
+    xs,
+    xr,
+    ys,
+    yr,
+    dxs,
+    dxr,
+    dys,
+    dyr,
+    ps,
+    pr,
+    hxs,
+    hxr,
+    hys,
+    hyr,
+    gxs,
+    gxr,
+    gys,
+    gyr,
+    ss,
+    sr,
+    ws,
+    wr,
+    ks,
+    kr,
+    pps,
+    ppr,
+    qqs,
+    qqr,
+):
+    ep, tp, nz, tok, width, cap, tok_a, kv_heads, group, units, columns, sunits = sizes
+    e = lax.axis_index("ep")
+    t = lax.axis_index("tp")
+    z, c = e // 2, e % 2
+    other = 1 - c
+    partner = z * 2 + other
+    tx, ty = t % 2, t // 2
+    xn = ty * 2 + (1 - tx)
+    yn = (1 - ty) * 2 + tx
+    dn = (1 - ty) * 2 + (1 - tx)
+    half = tok // 2
+    slots = 2 * cap
+    hcut = (slots // 2 + 15) // 16 * 16
+    row_c = pl.multiple_of(c * tok, 16)
+    row_o = pl.multiple_of(other * tok, 16)
+
+    def rc(src, dst, s_sem, r_sem, dev):
+        return pltpu.make_async_remote_copy(
+            src_ref=src,
+            dst_ref=dst,
+            send_sem=s_sem,
+            recv_sem=r_sem,
+            device_id=dev,
+            device_id_type=MESH,
+        )
+
+    unit0 = xbuf.at[z, t, pl.ds(row_c, tok), :]
+    loads = [
+        (x_hbm, unit0),
+        (wt_hbm, wbuf.at[e]),
+        (k_hbm, kbuf.at[pl.ds(WINDOW, tok_a), :]),
+        (v_hbm, vbuf.at[pl.ds(WINDOW, tok_a), :]),
+        (q_hbm, qbuf),
+        (gate_hbm.at[0], gate),
+        (up_hbm.at[0], up),
+        (sgate_hbm, sgate),
+        (sup_hbm, sup),
+        (down_hbm.at[0], down),
+        (sdown_hbm, sdown),
+    ]
+    copies = [
+        pltpu.make_async_copy(a, b, local_sem.at[i]) for i, (a, b) in enumerate(loads)
+    ]
+    for cp in copies:
+        cp.start()
+
+    barrier = pltpu.get_barrier_semaphore()
+    for d in range(1, ep):
+        pl.semaphore_signal(barrier, inc=1, device_id=((e + d) % ep, t), device_id_type=MESH)
+    for d in range(1, tp):
+        pl.semaphore_signal(barrier, inc=1, device_id=(e, (t + d) % tp), device_id_type=MESH)
+    pl.semaphore_wait(barrier, ep + tp - 2)
+
+    def unit(zi, ti, row, first=0, count=tok):
+        return xbuf.at[zi, ti, pl.ds(row + first, count), :]
+
+    def z_copy(d):
+        zi = (z + d) % nz
+        return rc(unit0, unit0, zs.at[d], zr.at[z], (zi * 2 + c, t))
+
+    def z_landed(zi):
+        u = unit(zi, t, row_c)
+        return rc(u, u, zs.at[0], zr.at[zi], (e, xn))
+
+    def x_copy(zi):
+        u = unit(zi, t, row_c)
+        return rc(u, u, xs.at[zi], xr.at[zi], (e, xn))
+
+    def y_copy(zi):
+        u = unit(zi, t, row_c)
+        return rc(u, u, ys.at[zi], yr.at[zi], (e, yn))
+
+    def x_landed(zi):
+        u = unit(zi, xn, row_c)
+        return rc(u, u, xs.at[zi], xr.at[zi], (e, xn))
+
+    def y_landed(zi):
+        u = unit(zi, yn, row_c)
+        return rc(u, u, ys.at[zi], yr.at[zi], (e, yn))
+
+    def dy_copy(zi):
+        u = unit(zi, xn, row_c, 0, half)
+        return rc(u, u, dys.at[zi], dyr.at[zi], (e, yn))
+
+    def dx_copy(zi):
+        u = unit(zi, yn, row_c, half, half)
+        return rc(u, u, dxs.at[zi], dxr.at[zi], (e, xn))
+
+    def dy_landed(zi):
+        u = unit(zi, dn, row_c, 0, half)
+        return rc(u, u, dys.at[zi], dyr.at[zi], (e, yn))
+
+    def dx_landed(zi):
+        u = unit(zi, dn, row_c, half, half)
+        return rc(u, u, dxs.at[zi], dxr.at[zi], (e, xn))
+
+    def p_copy(zi, ti):
+        u = unit(zi, ti, row_c)
+        return rc(u, u, ps.at[zi, ti], pr.at[zi, ti], (partner, t))
+
+    def p_landed(zi, ti):
+        u = unit(zi, ti, row_o)
+        return rc(u, u, ps.at[zi, ti], pr.at[zi, ti], (partner, t))
+
+    def hx_copy(zi):
+        u = hbuf.at[zi, t]
+        return rc(u, u, hxs.at[zi], hxr.at[zi], (e, xn))
+
+    def hy_copy(zi):
+        u = hbuf.at[zi, t]
+        return rc(u, u, hys.at[zi], hyr.at[zi], (e, yn))
+
+    def hx_landed(zi):
+        u = hbuf.at[zi, xn]
+        return rc(u, u, hxs.at[zi], hxr.at[zi], (e, xn))
+
+    def hy_landed(zi):
+        u = hbuf.at[zi, yn]
+        return rc(u, u, hys.at[zi], hyr.at[zi], (e, yn))
+
+    def gy_copy(zi):
+        u = hbuf.at[zi, xn, pl.ds(0, hcut), :]
+        return rc(u, u, gys.at[zi], gyr.at[zi], (e, yn))
+
+    def gx_copy(zi):
+        u = hbuf.at[zi, yn, pl.ds(hcut, slots - hcut), :]
+        return rc(u, u, gxs.at[zi], gxr.at[zi], (e, xn))
+
+    def gy_landed(zi):
+        u = hbuf.at[zi, dn, pl.ds(0, hcut), :]
+        return rc(u, u, gys.at[zi], gyr.at[zi], (e, yn))
+
+    def gx_landed(zi):
+        u = hbuf.at[zi, dn, pl.ds(hcut, slots - hcut), :]
+        return rc(u, u, gxs.at[zi], gxr.at[zi], (e, xn))
+
+    def s_copy(d):
+        u = shbuf.at[t]
+        return rc(u, u, ss.at[d], sr.at[t], (e, (t + d) % tp))
+
+    def s_landed(ti):
+        u = shbuf.at[ti]
+        return rc(u, u, ss.at[0], sr.at[ti], (e, xn))
+
+    def w_copy(d):
+        u = wbuf.at[e]
+        return rc(u, u, ws.at[d], wr.at[e], ((e + d) % ep, t))
+
+    def w_landed(ei):
+        u = wbuf.at[ei]
+        return rc(u, u, ws.at[0], wr.at[ei], (partner, t))
+
+    after, before = (e + 1) % ep, (e + ep - 1) % ep
+    tail = pl.ds(tok_a, WINDOW)
+    first = pl.ds(WINDOW, WINDOW)
+    low = pl.ds(0, WINDOW)
+    high = pl.ds(WINDOW + tok_a, WINDOW)
+    halos = [
+        rc(kbuf.at[tail, :], kbuf.at[low, :], ks.at[0], kr.at[0], (after, t)),
+        rc(kbuf.at[first, :], kbuf.at[high, :], ks.at[1], kr.at[1], (before, t)),
+        rc(vbuf.at[tail, :], vbuf.at[low, :], ks.at[2], kr.at[2], (after, t)),
+        rc(vbuf.at[first, :], vbuf.at[high, :], ks.at[3], kr.at[3], (before, t)),
+    ]
+
+    def pp_copy(zi):
+        return rc(pbuf.at[zi, other], prx.at[zi], pps.at[zi], ppr.at[zi], (partner, t))
+
+    def qq_copy(zi):
+        return rc(qtx.at[zi], qrx.at[z], qqs.at[zi], qqr.at[z], (zi * 2 + c, t))
+
+    def qq_landed(zi):
+        return rc(qrx.at[zi], qrx.at[zi], qqs.at[zi], qqr.at[zi], (partner, t))
+
+    copies[0].wait()
+    x_copy(z).start()
+    y_copy(z).start()
+    for d in range(1, nz):
+        z_copy(d).start()
+    p_copy(z, t).start()
+    copies[1].wait()
+    for d in range(1, ep):
+        w_copy(d).start()
+    copies[2].wait()
+    copies[3].wait()
+    for h in halos:
+        h.start()
+    copies[4].wait()
+
+    lane = lax.broadcasted_iota(jnp.int32, (WINDOW, LANES), 1)
+    leading = (lane % (HEAD_DIM // 2)) < HEAD_DIM // 4
+
+    def turn(block, head_gain, table_rows):
+        v = block.astype(F32)
+        v = v * lax.rsqrt(jnp.mean(v * v, axis=-1, keepdims=True) + epsilon) * head_gain
+        swapped = jnp.where(
+            leading,
+            pltpu.roll(v, HEAD_DIM - HEAD_DIM // 4, 1),
+            pltpu.roll(v, HEAD_DIM // 4, 1),
+        )
+        return (v * cos_ref[table_rows, :] + swapped * sin_ref[table_rows, :]).astype(BF16)
+
+    heads = kv_heads * group
+
+    def turn_q(i, carry):
+        rows = pl.ds(pl.multiple_of(i * WINDOW, WINDOW), WINDOW)
+        table = pl.ds(pl.multiple_of((i + 1) * WINDOW, WINDOW), WINDOW)
+        for h in range(heads):
+            cols = slice(h * HEAD_DIM, (h + 1) * HEAD_DIM)
+            qbuf[rows, cols] = turn(qbuf[rows, cols], qgain_ref[...], table)
+        return carry
+
+    nq = tok_a // WINDOW
+    lax.fori_loop(0, nq, turn_q, 0)
+
+    def forward_z(zi):
+        z_landed(zi).wait_recv()
+        x_copy(zi).start()
+        y_copy(zi).start()
+        p_copy(zi, t).start()
+
+    forward_z((z + 1) % nz)
+
+    for h in halos:
+        h.wait()
+
+    def turn_k(i, carry):
+        rows = pl.ds(pl.multiple_of(i * WINDOW, WINDOW), WINDOW)
+        for h in range(kv_heads):
+            cols = slice(h * HEAD_DIM, (h + 1) * HEAD_DIM)
+            kbuf[rows, cols] = turn(kbuf[rows, cols], kgain_ref[...], rows)
+        return carry
+
+    lax.fori_loop(0, nq + 2, turn_k, 0)
+    for d in range(1, ep):
+        w_landed((e + d) % ep).wait_recv()
+    for cp in copies[5:]:
+        cp.wait()
+
+    span = 3 * WINDOW
+
+    def attend(i, carry):
+        qb, kh = i // kv_heads, i % kv_heads
+        rows = pl.ds(pl.multiple_of(qb * WINDOW, WINDOW), WINDOW)
+        keys = pl.ds(pl.multiple_of(qb * WINDOW, WINDOW), span)
+        kcols = pl.ds(pl.multiple_of(kh * HEAD_DIM, HEAD_DIM), HEAD_DIM)
+        near = lax.broadcasted_iota(jnp.int32, (WINDOW, span), 1)
+        mine = lax.broadcasted_iota(jnp.int32, (WINDOW, span), 0)
+        pos = e * tok_a + (qb - 1) * WINDOW + near
+        inside = (
+            (near - mine >= 0) & (near - mine <= 2 * WINDOW) & (pos >= 0) & (pos < ep * tok_a)
+        )
+        kk = kbuf[keys, kcols]
+        vv = vbuf[keys, kcols]
+        for g in range(group):
+            qcols = pl.ds(
+                pl.multiple_of((kh * group + g) * HEAD_DIM, HEAD_DIM), HEAD_DIM
+            )
+            scores = lax.dot_general(
+                qbuf[rows, qcols], kk, (((1,), (1,)), ((), ())), preferred_element_type=F32
+            )
+            raised = jnp.where(inside, jnp.exp(scores * HEAD_DIM ** (-0.5)), 0.0)
+            sink = jnp.exp(sink_ref[kh * group + g])
+            total = jnp.sum(raised, axis=-1, keepdims=True) + sink[0:1, 0:1]
+            weights = (raised * (1.0 / total)).astype(BF16)
+            att_ref[rows, qcols] = jnp.dot(weights, vv, preferred_element_type=F32).astype(BF16)
+        return carry
+
+    upper = (
+        lax.broadcasted_iota(jnp.int32, (tok, tok), 0)
+        < lax.broadcasted_iota(jnp.int32, (tok, tok), 1)
+    ).astype(F32)
+
+    def picks(block):
+        weight = wbuf[block, pl.ds(e, 1), :][:, :tok]
+        named = jnp.where(weight > 0.0, 1.0, 0.0)
+        rank = jnp.dot(
+            jnp.broadcast_to(named, (16, tok)).astype(BF16),
+            upper.astype(BF16),
+            preferred_element_type=F32,
+        )[0:1, :]
+        slot = lax.broadcasted_iota(jnp.int32, (cap, tok), 0).astype(F32)
+        hot = jnp.where((slot == rank) & (named > 0.0), 1.0, 0.0)
+        return hot, jnp.sum(hot * weight, axis=1, keepdims=True)
+
+    chunk = 32
+
+    def silu_pair(g, u, f):
+        g = g * f
+        return g / (1.0 + jnp.exp(-g)) * (u * f)
+
+    tile = min(256, units)
+
+    def project_pair(zi):
+        def scale(i, carry):
+            rows = pl.ds(pl.multiple_of(i * chunk, chunk), chunk)
+            squares = jnp.zeros((chunk, 1), F32)
+            for ti in range(tp):
+                v = xbuf[zi, ti, rows, :].astype(F32)
+                squares += jnp.sum(v * v, axis=1, keepdims=True)
+                cols = slice(ti * width, (ti + 1) * width)
+                scaled[rows, cols] = (v * gain_ref[:, cols]).astype(BF16)
+            f = lax.rsqrt(squares / (tp * width) + epsilon)
+            factor[rows, :] = jnp.broadcast_to(f, (chunk, LANES))
+            return carry
+
+        lax.fori_loop(0, 2 * tok // chunk, scale, 0)
+
+        def columns_of(n, carry):
+            cols = pl.ds(pl.multiple_of(n * tile, tile), tile)
+            g = jnp.dot(scaled[...], gate[:, cols], preferred_element_type=F32)
+            u = jnp.dot(scaled[...], up[:, cols], preferred_element_type=F32)
+            hid[:, cols] = silu_pair(g, u, factor[:, 0:1]).astype(BF16)
+            return carry
+
+        lax.fori_loop(0, units // tile, columns_of, 0)
+        parts = []
+        for ci in range(2):
+            hot, _ = picks(zi * 2 + ci)
+            parts.append(
+                jnp.dot(
+                    hot.astype(BF16),
+                    hid[ci * tok : (ci + 1) * tok, :],
+                    preferred_element_type=F32,
+                )
+            )
+        hbuf[zi, t] = jnp.concatenate(parts, axis=0).astype(BF16)
+
+    def shared_up():
+        rows = pl.ds(row_c, tok)
+        g = jnp.dot(scaled[rows, :], sgate[...], preferred_element_type=F32)
+        u = jnp.dot(scaled[rows, :], sup[...], preferred_element_type=F32)
+        shbuf[t] = silu_pair(g, u, factor[rows, 0:1]).astype(BF16)
+
+    ctile = min(256, columns)
+
+    def down_pair(zi):
+        picked = [picks(zi * 2 + ci) for ci in range(2)]
+        slot_weight = jnp.concatenate([p[1] for p in picked], axis=0)
+
+        def columns_of(n, carry):
+            cols = pl.ds(pl.multiple_of(n * ctile, ctile), ctile)
+            acc = jnp.zeros((slots, ctile), F32)
+            for ti in range(tp):
+                acc += jnp.dot(
+                    hbuf[zi, ti],
+                    down[ti * units : (ti + 1) * units, cols],
+                    preferred_element_type=F32,
+                )
+            weighted = acc.astype(BF16).astype(F32) * slot_weight
+            for ci in range(2):
+                spread = lax.dot_general(
+                    picked[ci][0].astype(BF16),
+                    weighted[ci * cap : (ci + 1) * cap, :].astype(BF16),
+                    (((0,), (0,)), ((), ())),
+                    preferred_element_type=F32,
+                )
+                pbuf[zi, ci, :, cols] = spread.astype(BF16)
+            return carry
+
+        lax.fori_loop(0, columns // ctile, columns_of, 0)
+
+    per_step = nq * kv_heads // nz
+
+    def step(s, carry):
+        @pl.when(s < nz)
+        def _():
+            lax.fori_loop(s * per_step, (s + 1) * per_step, attend, 0)
+            zi = (z + s) % nz
+            x_landed(zi).wait_recv()
+            dy_copy(zi).start()
+            p_copy(zi, xn).start()
+            y_landed(zi).wait_recv()
+            dx_copy(zi).start()
+            p_copy(zi, yn).start()
+
+            @pl.when(s + 2 < nz)
+            def _():
+                forward_z((z + s + 2) % nz)
+
+            dy_landed(zi).wait_recv()
+            dx_landed(zi).wait_recv()
+            p_copy(zi, dn).start()
+            for ti in range(tp):
+                p_landed(zi, ti).wait_recv()
+            project_pair(zi)
+            hx_copy(zi).start()
+            hy_copy(zi).start()
+
+            @pl.when(s == 0)
+            def _():
+                shared_up()
+                for d in range(1, tp):
+                    s_copy(d).start()
+
+        @pl.when((s >= 1) & (s < nz + 1))
+        def _():
+            zi = (z + s - 1) % nz
+            hx_landed(zi).wait_recv()
+            gy_copy(zi).start()
+            hy_landed(zi).wait_recv()
+            gx_copy(zi).start()
+
+        @pl.when((s >= 2) & (s < nz + 2))
+        def _():
+            zi = (z + s - 2) % nz
+            gy_landed(zi).wait_recv()
+            gx_landed(zi).wait_recv()
+            down_pair(zi)
+            pp_copy(zi).start()
+            pp_copy(zi).wait_recv()
+            qtx[zi] = (pbuf[zi, c].astype(F32) + prx[zi].astype(F32)).astype(BF16)
+
+            @pl.when(s > 2)
+            def _():
+                qq_copy(zi).start()
+
+        return carry
+
+    lax.fori_loop(0, nz + 2, step, 0)
+
+    for d in range(1, tp):
+        s_landed((t + d) % tp).wait_recv()
+    for d in range(1, nz):
+        qq_landed((z + d) % nz).wait_recv()
+    for n in range(columns // ctile):
+        cols = slice(n * ctile, (n + 1) * ctile)
+        acc = qtx[z, :, cols].astype(F32)
+        for d in range(1, nz):
+            acc += qrx[(z + d) % nz, :, cols].astype(F32)
+        for ti in range(tp):
+            acc += jnp.dot(
+                shbuf[ti],
+                sdown[ti * sunits : (ti + 1) * sunits, cols],
+                preferred_element_type=F32,
+            )
+        out_ref[:, cols] = acc.astype(BF16)
+
+    for d in range(1, nz):
+        z_copy(d).wait_send()
+        qq_copy((z + d) % nz).wait_send()
+    for d in range(1, tp):
+        s_copy(d).wait_send()
+    for d in range(1, ep):
+        w_copy(d).wait_send()
+
+    def drain(zi, carry):
+        for kind in (x_copy, y_copy, dx_copy, dy_copy, hx_copy, hy_copy, gx_copy, gy_copy, pp_copy):
+            kind(zi).wait_send()
+        for ti in range(tp):
+            p_copy(zi, ti).wait_send()
+        return carry
+
+    lax.fori_loop(0, nz, drain, 0)
+
+
+def fast_shards(
+    query_vectors,
+    key_vectors,
+    value_vectors,
+    query_gain,
+    key_gain,
+    sink_logits,
+    moe_rows,
+    norm_gain,
+    expert_ids,
+    route_weights,
+    expert_gate,
+    expert_up,
+    expert_down,
+    shared_gate,
+    shared_up,
+    shared_down,
+):
+    ep, tp = lax.axis_size("ep"), lax.axis_size("tp")
+    nz = ep // 2
+    tok, width = moe_rows.shape
+    cap = max(2, 3 * tok * TOP_K // (2 * ep))
+    tok_a = query_vectors.shape[0]
+    heads = sink_logits.shape[0]
+    kv_heads = key_vectors.shape[1] // HEAD_DIM
+    group = heads // kv_heads
+    units = expert_gate.shape[2]
+    columns = expert_down.shape[2]
+    sunits = shared_gate.shape[1]
+    sizes = (ep, tp, nz, tok, width, cap, tok_a, kv_heads, group, units, columns, sunits)
+    full = tp * width
+
+    extent = tok_a + 2 * WINDOW
+    positions = lax.axis_index("ep") * tok_a - WINDOW + jnp.arange(extent, dtype=jnp.int32)
+    quarter = HEAD_DIM // 4
+    inverse = rotary_base ** (-4.0 * jnp.arange(quarter, dtype=jnp.int32).astype(F32) / HEAD_DIM)
+    grid_row = (positions // GRID_W).astype(F32)[:, None] * inverse
+    grid_col = (positions % GRID_W).astype(F32)[:, None] * inverse
+    cr, cc, sr, sc = jnp.cos(grid_row), jnp.cos(grid_col), jnp.sin(grid_row), jnp.sin(grid_col)
+    cos = jnp.concatenate([cr, cr, cc, cc], axis=-1)
+    sin = jnp.concatenate([-sr, sr, -sc, sc], axis=-1)
+
+    experts = jnp.arange(ep, dtype=jnp.int32)
+    table = jnp.sum(
+        jnp.where(expert_ids.T[None, :, :] == experts[:, None, None], route_weights.T[None], 0.0),
+        axis=1,
+    )
+    padded_tok = (tok + LANES - 1) // LANES * LANES
+    table = jnp.pad(table, ((0, 0), (0, padded_tok - tok)))
+    sinks = jnp.broadcast_to(sink_logits[:, None, None], (heads, 8, LANES))
+
+    vm = pl.BlockSpec(memory_space=pltpu.VMEM)
+    hb = pl.BlockSpec(memory_space=pl.ANY)
+    dma = pltpu.SemaphoreType.DMA
+    slots = 2 * cap
+    zz = [dma((nz,))] * 2
+    return pl.pallas_call(
+        functools.partial(moe_kernel, sizes),
+        out_shape=(
+            jax.ShapeDtypeStruct((tok_a, heads * HEAD_DIM), BF16),
+            jax.ShapeDtypeStruct((tok, columns), BF16),
+        ),
+        in_specs=[hb, hb, hb, vm, vm, vm, vm, vm, hb, vm, hb, hb, hb, hb, hb, hb, hb],
+        out_specs=(vm, vm),
+        scratch_shapes=[
+            pltpu.VMEM((nz, tp, 2 * tok, width), BF16),
+            pltpu.VMEM((full, units), BF16),
+            pltpu.VMEM((full, units), BF16),
+            pltpu.VMEM((tp * units, columns), BF16),
+            pltpu.VMEM((full, sunits), BF16),
+            pltpu.VMEM((full, sunits), BF16),
+            pltpu.VMEM((tp * sunits, columns), BF16),
+            pltpu.VMEM((tok_a, heads * HEAD_DIM), BF16),
+            pltpu.VMEM((extent, kv_heads * HEAD_DIM), BF16),
+            pltpu.VMEM((extent, kv_heads * HEAD_DIM), BF16),
+            pltpu.VMEM((ep, ep, padded_tok), F32),
+            pltpu.VMEM((2 * tok, full), BF16),
+            pltpu.VMEM((2 * tok, LANES), F32),
+            pltpu.VMEM((2 * tok, units), BF16),
+            pltpu.VMEM((nz, tp, slots, units), BF16),
+            pltpu.VMEM((tp, tok, sunits), BF16),
+            pltpu.VMEM((nz, 2, tok, columns), BF16),
+            pltpu.VMEM((nz, tok, columns), BF16),
+            pltpu.VMEM((nz, tok, columns), BF16),
+            pltpu.VMEM((nz, tok, columns), BF16),
+            dma((11,)),
+        ]
+        + zz * 5
+        + [dma((nz, tp))] * 2
+        + zz * 4
+        + [dma((tp,))] * 2
+        + [dma((ep,))] * 2
+        + [dma((4,))] * 2
+        + zz * 2,
+        compiler_params=pltpu.CompilerParams(
+            collective_id=0, has_side_effects=True, vmem_limit_bytes=60 * 1024 * 1024
+        ),
+    )(
+        query_vectors,
+        key_vectors,
+        value_vectors,
+        cos,
+        sin,
+        query_gain[None, :],
+        key_gain[None, :],
+        sinks,
+        moe_rows,
+        norm_gain[None, :],
+        table,
+        expert_gate,
+        expert_up,
+        expert_down,
+        shared_gate,
+        shared_up,
+        shared_down,
+    )
+
+
+def choose(*args):
+    ep, tp = lax.axis_size("ep"), lax.axis_size("tp")
+    query, rows = args[0], args[6]
+    kv_heads = args[1].shape[1] // HEAD_DIM
+    tok, width = rows.shape
+    cap = max(2, 3 * tok * TOP_K // (2 * ep))
+    gathered = ep * tok * tp * width * 2
+    chunks = query.shape[0] // WINDOW * kv_heads
+    fits = (
+        gathered <= 16 * 1024 * 1024
+        and tp == 4
+        and ep % 2 == 0
+        and tok % 32 == 0
+        and (2 * cap) % 16 == 0
+        and cap % 8 == 0
+        and chunks % (ep // 2) == 0
+    )
+    return fast_shards(*args) if fits else shards(*args)
+
+
 def solution(mesh):
     placed = (
         P("ep", "tp"),
@@ -204,7 +880,7 @@
         P(None, "tp"),
     )
     return jax.shard_map(
-        shards,
+        choose,
         mesh=mesh,
         in_specs=placed,
         out_specs=(P("ep", "tp"), P("ep", "tp")),

time: 299 us -> 167 us (0.56)
  waiting for transfers between devices: 174 us -> 0 us
  Pallas kernels: 0 us -> 155 us
  matrix products: 34.9 us -> 0 us
  local copies, waits for them, and re-layouts: 35.3 us -> 5.28 us
  other arithmetic: 23.4 us -> 5.09 us
  starting transfers between devices: 16.2 us -> 0 us
  between operations: 14.3 us -> 0.69 us
    pallas_call x0 -> x1, Pallas kernels: none -> 155 us  [fast_shards(): pl.pallas_call(functools.partial(moe_kernel, sizes), out_shape=(jax.Shape...]
    all_gather x3 -> x0, waiting for transfers between devices: 101 us -> none  [the longest x1 77.6 us: shards(): lax.all_gather(arrived, 'tp', axis=1, tiled=True)]
    all_to_all x2 -> x0, waiting for transfers between devices: 73 us -> none  [the longest x1 45.4 us: shards(): lax.all_to_all(outgoing.reshape(ep_size, capacity, width_here), 'ep', spl...]
    dot_general x8 -> x0, matrix products: 34.9 us -> none  [the longest x1 8.88 us: shards(): jnp.dot(portion[:slots_all], local_down, preferred_element_type=jnp.float32)]
    all_to_all x2 -> x0, starting transfers between devices: 11.1 us -> none  [the longest x1 6.35 us: shards(): lax.all_to_all(outgoing.reshape(ep_size, capacity, width_here), 'ep', spl...]
    gather x3 -> x0, local copies, waits for them, and re-layouts: 10.3 us -> none  [the longest x2 6.12 us: shards(): jnp.take(returned, target, axis=0).reshape(tokens_here, TOP_K, columns)]
    reduce_sum x7 -> x1, other arithmetic: 10.2 us -> 0.01 us  [fast_shards(): jnp.sum(jnp.where(expert_ids.T[None, :, :] == experts[:, None, None], rou...]
    concatenate x4 -> x0, local copies, waits for them, and re-layouts: 7.81 us -> none  [rotate_heads(): jnp.concatenate([half_turn(row_half), half_turn(col_half)], axis=-1)]
  transfers between devices with their start and end apart: 7 -> 0, of which waited for: 4 -> 0; matrix products, arithmetic and copies ran while one was open for 18% -> 0% of each run, Pallas kernels for 0% -> 0%
where the time goes in v1:
time: 167 us; the launch traced here: 166 us
  Pallas kernels  155 us (93%)
  local copies, waits for them, and re-layouts  5.28 us (3%)
  other arithmetic  5.09 us (3%)
    pallas_call x1, Pallas kernels, fast_shards(): pl.pallas_call(functools.partial(moe_kernel, sizes), out_shape=(jax.Shape...  155 us
    unnamed x8, local copies, waits for them, and re-layouts  3.99 us

profile of v1, /device:TPU:0, one launch (start us, length us, event | category | flops | bytes accessed | tf_op | source)
XLA Modules:
  0.0 166.4 jit_solution(17437244332311485371)
XLA Ops:
  0.6 0.0 copy-start.2
  0.6 0.0 copy-start.1
  0.7 0.0 copy-start
  0.7 2.8 %fusion = (f32[768,32]{1,0:T(8,128)S(1)}, f32[768,32]{1,0:T(8,128)S(1)}, f32[768,32]{1,0:T(8,128)S(1)}, f32[768,32]{1,0:T(8,128)S(1)}, f32[768,32]{1,0:T(8,128)S(1)}, /*index=5*/f32[768,32]{1,0:T(8,128)S(1)}) fusion(f32[32]{0:T(128)S(1)} %multiply_power_fusion, f32[768]{0:T(1024)S(1)} %get-tuple-element.11, f32[768]{0:T(1024)S(1)} %get-tuple-element.12), kind=kLoop, calls=%fused_computation.6 | loop fusion | flops 98304 | bytes 596096 | tf_op jit(solution)/shard_map/neg | solution.py:765
  3.5 1.1 pad_maximum_fusion.1.sin_ref
  4.6 1.1 pad_maximum_fusion.cos_ref
  5.8 0.0 copy-done.2
  5.8 0.7 broadcast_in_dim.36.sink_ref
  6.5 0.0 copy-done.1
  6.5 0.0 copy-done
  6.5 0.6 pad.4.wt_hbm
  7.1 155.4 %shard_map.167 = (bf16[512,1024]{1,0:T(8,128)(2,1)}, bf16[160,1024]{1,0:T(8,128)(2,1)}) custom-call(bf16[512,1024]{1,0:T(8,128)(2,1)} %q_hbm.1, bf16[512,512]{1,0:T(8,128)(2,1)} %k_hbm.1, bf16[512,512]{1,0:T(8,128)(2,1)} %v_hbm.1, f32[768,128]{1,0:T(8,128)} %pad_maximum_fusion.cos_ref, f32[768,128]{1,0:T(8,128)} %pad_maximum_fusion.1.sin_ref, ...), custom_call_target="tpu_custom_call" | custom-call | tf_op jit(solution)/shard_map/pallas_call | solution.py:781
  162.4 2.3 %copy.22 = bf16[512,1024]{1,0:T(8,128)(2,1)} copy(bf16[512,1024]{1,0:T(8,128)(2,1)} %get-tuple-element.15) | data formatting | bytes 2097152
  164.7 1.7 %copy.23 = bf16[160,1024]{1,0:T(8,128)(2,1)} copy(bf16[160,1024]{1,0:T(8,128)(2,1)} %get-tuple-element.16) | data formatting | bytes 655360
  (3 shorter events, 0.0 us)
Async XLA Ops:
  0.6 5.1 %copy-start.2 = (f32[8]{0:T(128)S(1)}, f32[8]{0:T(128)}, u32[]{:S(2)}) copy-start(f32[8]{0:T(128)} %param.21) | copy-start | bytes 100
  0.6 5.8 %copy-start.1 = (s32[160,4]{0,1:T(4,128)S(1)}, s32[160,4]{0,1:T(4,128)}, u32[]{:S(2)}) copy-start(s32[160,4]{0,1:T(4,128)} %param.24) | copy-start | bytes 7684
  0.7 5.8 %copy-start = (f32[160,4]{0,1:T(4,128)S(1)}, f32[160,4]{0,1:T(4,128)}, u32[]{:S(2)}) copy-start(f32[160,4]{0,1:T(4,128)} %param.25) | copy-start | bytes 7684

commit v2 on v1

--- a/solution.py
+++ b/solution.py
@@ -755,12 +755,22 @@
     full = tp * width
 
     extent = tok_a + 2 * WINDOW
-    positions = lax.axis_index("ep") * tok_a - WINDOW + jnp.arange(extent, dtype=jnp.int32)
+    first_row = (lax.axis_index("ep") * tok_a - WINDOW) // GRID_W
+    grid_rows = extent // GRID_W
     quarter = HEAD_DIM // 4
     inverse = rotary_base ** (-4.0 * jnp.arange(quarter, dtype=jnp.int32).astype(F32) / HEAD_DIM)
-    grid_row = (positions // GRID_W).astype(F32)[:, None] * inverse
-    grid_col = (positions % GRID_W).astype(F32)[:, None] * inverse
-    cr, cc, sr, sc = jnp.cos(grid_row), jnp.cos(grid_col), jnp.sin(grid_row), jnp.sin(grid_col)
+    row_ids = first_row + jnp.arange(grid_rows, dtype=jnp.int32)
+    grid_row = row_ids.astype(F32)[:, None] * inverse
+    grid_col = jnp.arange(GRID_W, dtype=jnp.int32).astype(F32)[:, None] * inverse
+
+    def by_row(a):
+        return jnp.broadcast_to(a[:, None, :], (grid_rows, GRID_W, quarter)).reshape(extent, quarter)
+
+    def by_col(a):
+        return jnp.broadcast_to(a[None], (grid_rows, GRID_W, quarter)).reshape(extent, quarter)
+
+    cr, sr = by_row(jnp.cos(grid_row)), by_row(jnp.sin(grid_row))
+    cc, sc = by_col(jnp.cos(grid_col)), by_col(jnp.sin(grid_col))
     cos = jnp.concatenate([cr, cr, cc, cc], axis=-1)
     sin = jnp.concatenate([-sr, sr, -sc, sc], axis=-1)
 
@@ -855,6 +865,7 @@
         and tok % 32 == 0
         and (2 * cap) % 16 == 0
         and cap % 8 == 0
+        and query.shape[0] % GRID_W == 0
         and chunks % (ep // 2) == 0
     )
     return fast_shards(*args) if fits else shards(*args)

time: 167 us -> 166 us (level)
  other arithmetic: 5.09 us -> 3.34 us
    neg x1, other arithmetic: 2.81 us -> 0.05 us  [fast_shards(): sin = jnp.concatenate([-sr, sr, -sc, sc], axis=-1)]
    unnamed x8 -> x2, local copies, waits for them, and re-layouts: 3.99 us -> 3.98 us
where the time goes in v2:
time: 166 us; the launch traced here: 165 us
  Pallas kernels  155 us (93%)
  local copies, waits for them, and re-layouts  6.05 us (4%)
  other arithmetic  3.34 us (2%)
    pallas_call x1, Pallas kernels, fast_shards(): pl.pallas_call(functools.partial(moe_kernel, sizes), out_shape=(jax.Shape...  155 us
    unnamed x2, local copies, waits for them, and re-layouts  3.98 us

profile of v2, /device:TPU:0, one launch (start us, length us, event | category | flops | bytes accessed | tf_op | source)
XLA Modules:
  0.0 165.5 jit_solution(14399645126841926587)
XLA Ops:
  0.7 0.7 select_reduce_fusion
  1.4 0.6 pad.4.wt_hbm
  2.0 0.1 multiply_sine_fusion.1
  2.1 1.3 broadcast_in_dim.68.sink_ref
  3.5 0.2 multiply_sine_fusion
  3.8 1.1 pad_maximum_fusion.cos_ref
  4.9 0.1 bitcast_negate_fusion
  5.0 1.1 pad_maximum_fusion.1.sin_ref
  6.1 155.3 %shard_map.167 = (bf16[512,1024]{1,0:T(8,128)(2,1)}, bf16[160,1024]{1,0:T(8,128)(2,1)}) custom-call(bf16[512,1024]{1,0:T(8,128)(2,1)} %q_hbm.1, bf16[512,512]{1,0:T(8,128)(2,1)} %k_hbm.1, bf16[512,512]{1,0:T(8,128)(2,1)} %v_hbm.1, f32[768,128]{1,0:T(8,128)} %pad_maximum_fusion.cos_ref, f32[768,128]{1,0:T(8,128)} %pad_maximum_fusion.1.sin_ref, ...), custom_call_target="tpu_custom_call" | custom-call | tf_op jit(solution)/shard_map/pallas_call | solution.py:791
  161.5 2.3 %copy.20 = bf16[512,1024]{1,0:T(8,128)(2,1)} copy(bf16[512,1024]{1,0:T(8,128)(2,1)} %get-tuple-element.10) | data formatting | bytes 2097152
  163.8 1.7 %copy.21 = bf16[160,1024]{1,0:T(8,128)(2,1)} copy(bf16[160,1024]{1,0:T(8,128)(2,1)} %get-tuple-element.11) | data formatting | bytes 655360
  (7 shorter events, 0.1 us)
